TPU v7x, 32 devices: a whole 2x2x4 slice. The times are simulated.
32 devices in a mesh: ep: 16 (over z, y, x), tp: 2 (over core).
Axes of the slice: x: 2, y: 2, z: 4, core: 2. Of those that a mesh axis runs over, the one named last changes fastest.
Arguments:
- tokens: bfloat16 [256, 2048], P(('ep', 'tp')), may hold values from -6 to 6
- mix_gain: float32 [2048], replicated, may hold values from 0.1 to 1.9
- w_query: bfloat16 [2048, 16, 128], P(None, 'tp', 'ep'), may hold values from -0.125 to 0.125
- w_key: bfloat16 [2048, 16, 128], P(None, 'tp', 'ep'), may hold values from -0.125 to 0.125
- w_value: bfloat16 [2048, 16, 128], P(None, 'tp', 'ep'), may hold values from -0.125 to 0.125
- w_zgate: bfloat16 [2048, 16, 128], P(None, 'tp', 'ep'), may hold values from -0.125 to 0.125
- w_beta: bfloat16 [2048, 16], P(None, 'tp'), may hold values from -0.125 to 0.125
- w_decay: bfloat16 [2048, 16], P(None, 'tp'), may hold values from -0.125 to 0.125
- decay_rate: float32 [16], P('tp'), may hold values from 0.5 to 8
- decay_bias: float32 [16], P('tp'), may hold values from -3 to 0
- head_gain: float32 [128], replicated, may hold values from 0.1 to 1.9
- state: float32 [256, 16, 128, 128], P('ep', 'tp'), may hold values from -1.5 to 1.5
- w_out: bfloat16 [2048, 2048], P('tp', 'ep'), may hold values from -0.125 to 0.125
- moe_gain: float32 [2048], replicated, may hold values from 0.1 to 1.9
- dense_mix: bfloat16 [2048], replicated, may hold values from -0.125 to 0.125
- dense_gate: bfloat16 [2048, 4096], P(None, ('ep', 'tp')), may hold values from -0.125 to 0.125
- dense_up: bfloat16 [2048, 4096], P(None, ('ep', 'tp')), may hold values from -0.125 to 0.125
- dense_down: bfloat16 [4096, 2048], P(('ep', 'tp')), may hold values from -0.09375 to 0.09375
- expert_gate: bfloat16 [16, 2048, 1024], P('ep', None, 'tp'), may hold values from -0.125 to 0.125
- expert_up: bfloat16 [16, 2048, 1024], P('ep', None, 'tp'), may hold values from -0.125 to 0.125
- expert_down: bfloat16 [16, 1024, 2048], P('ep', 'tp'), may hold values from -0.1875 to 0.1875
- expert_ids: int32 [256, 4], replicated, may hold values from 0 to 15, as said below
- route_weight: float32 [256, 4], replicated, may hold values from 0.1 to 1
Outputs:
- layer_out: bfloat16 [256, 2048], P(('ep', 'tp'))
- new_state: float32 [256, 16, 128, 128], P('ep', 'tp')
Inputs may be any that keep to these rules, and one draw needn't show every extreme that they name: `expert_ids`: the 4 experts of a row are distinct and lie in one group of 8 consecutive ids. In each aligned block of 16 rows (the rows of one index of ep) no expert is named by more than 8 rows, and at most 16 rows pick one group.
All inputs are finite; a program needn't handle non-finite values.
Results may differ from a plain program's by a relative error of at most 0.012.
Values may be sent and summed in bfloat16 or wider, within the bound.
A program may use at most 128 MiB of HBM per device.

v0:
```python
import jax
import jax.numpy as jnp
from jax import lax
from jax.sharding import PartitionSpec as P

EPG = 8


EPS = 1e-06


def rms_scale(values, gain):
    return values * lax.rsqrt(jnp.mean(values * values, axis=-1, keepdims=True) + EPS) * gain


def unit_rows(values):
    return values * lax.rsqrt(jnp.sum(values * values, axis=-1, keepdims=True) + EPS)


def body(
    tokens,
    mix_gain,
    w_query,
    w_key,
    w_value,
    w_zgate,
    w_beta,
    w_decay,
    decay_rate,
    decay_bias,
    head_gain,
    state,
    w_out,
    moe_gain,
    dense_mix,
    dense_gate,
    dense_up,
    dense_down,
    expert_gate,
    expert_up,
    expert_down,
    expert_ids,
    route_weight,
):
    ep_count = lax.axis_size("ep")
    tp_count = lax.axis_size("tp")
    group_idx = lax.axis_index("ep")
    own_rows = tokens.shape[0]
    tok_float = tokens.astype(jnp.float32)
    normed = rms_scale(tok_float, mix_gain).astype(jnp.bfloat16)
    rows_all = lax.all_gather(normed, ("ep", "tp"), axis=0, tiled=True)
    total_rows = rows_all.shape[0]
    seq_group = total_rows // ep_count
    w_cat = jnp.stack([w_query, w_key, w_value, w_zgate], axis=1)
    model_width = w_cat.shape[0]
    local_heads = w_cat.shape[2]
    head_slice = w_cat.shape[3]
    projected = jnp.dot(
        rows_all, w_cat.reshape(model_width, -1), preferred_element_type=jnp.float32
    )
    projected = projected.astype(jnp.bfloat16).reshape(total_rows, 4, local_heads, head_slice)
    by_heads = lax.all_to_all(projected, "ep", split_axis=0, concat_axis=3, tiled=True).astype(
        jnp.float32
    )
    head_size = by_heads.shape[3]
    query = unit_rows(jax.nn.silu(by_heads[:, 0])) * head_size ** (-0.5)
    key_vec = unit_rows(jax.nn.silu(by_heads[:, 1]))
    value = jax.nn.silu(by_heads[:, 2])
    gate_in = by_heads[:, 3]
    seq_rows = lax.dynamic_slice_in_dim(rows_all, group_idx * seq_group, seq_group, 0)
    beta_rate = jax.nn.sigmoid(jnp.dot(seq_rows, w_beta, preferred_element_type=jnp.float32))
    decay_in = jnp.dot(seq_rows, w_decay, preferred_element_type=jnp.float32)
    retain = jnp.exp(-decay_rate * jax.nn.softplus(decay_in + decay_bias))
    recalled = jnp.einsum("shkv,shk->shv", state, key_vec, precision=lax.Precision.HIGHEST)
    correction = value - retain[..., None] * recalled
    new_state = (
        retain[..., None, None] * state
        + (beta_rate[..., None] * key_vec)[..., :, None] * correction[..., None, :]
    )
    readout = jnp.einsum("shkv,shk->shv", new_state, query, precision=lax.Precision.HIGHEST)
    gated = rms_scale(readout, head_gain) * jax.nn.silu(gate_in)
    gated = gated.astype(jnp.bfloat16).reshape(seq_group, local_heads * head_size)
    partial_value = jnp.dot(
        lax.all_gather(gated, "ep", axis=0, tiled=True), w_out, preferred_element_type=jnp.float32
    )
    partial_value = partial_value.reshape(ep_count, tp_count, own_rows, partial_value.shape[1])
    partial_value = lax.psum_scatter(
        partial_value.astype(jnp.bfloat16), "tp", scatter_dimension=1, tiled=True
    ).astype(jnp.float32)
    mixed = (
        lax.all_to_all(
            partial_value.astype(jnp.bfloat16), "ep", split_axis=0, concat_axis=3, tiled=True
        )
        .astype(partial_value.dtype)
        .reshape(own_rows, -1)
    )
    resid = tok_float + mixed
    moe_in = rms_scale(resid, moe_gain).astype(jnp.bfloat16)
    moe_all = lax.all_gather(moe_in, ("ep", "tp"), axis=0, tiled=True)
    dense_hidden = (
        jax.nn.silu(jnp.dot(moe_all, dense_gate, preferred_element_type=jnp.float32))
        * jnp.dot(moe_all, dense_up, preferred_element_type=jnp.float32)
    ).astype(jnp.bfloat16)
    mix_factor = jax.nn.sigmoid(jnp.dot(moe_all, dense_mix, preferred_element_type=jnp.float32))
    top_count = expert_ids.shape[1]
    group_count = ep_count // EPG
    group_cap = min(seq_group, 2 * seq_group // group_count)
    capacity = (group_cap * top_count + EPG - 1) // EPG
    slot_count = ep_count * capacity
    positions = jnp.arange(total_rows, dtype=jnp.int32)
    block_idx = positions // seq_group
    matched = expert_ids == group_idx
    routed = jnp.any(matched, axis=1).astype(jnp.int32)
    weight = jnp.sum(jnp.where(matched, route_weight, 0.0), axis=1)
    rank_in = jnp.cumsum(routed.reshape(-1, seq_group), axis=1).reshape(-1) - routed
    slot_idx = block_idx * capacity + rank_in
    slot_iota = jnp.arange(slot_count, dtype=jnp.int32)
    matches = (slot_idx[None, :] == slot_iota[:, None]) & (routed[None, :] > 0)
    source = jnp.sum(jnp.where(matches, positions[None, :], 0), axis=1)
    picked = jnp.take(moe_all, source, axis=0)
    expert_hidden = (
        jax.nn.silu(jnp.dot(picked, expert_gate[0], preferred_element_type=jnp.float32))
        * jnp.dot(picked, expert_up[0], preferred_element_type=jnp.float32)
    ).astype(jnp.bfloat16)
    expert_out = jnp.dot(expert_hidden, expert_down[0], preferred_element_type=jnp.float32)
    slot_clip = jnp.minimum(slot_idx, slot_count - 1)
    moe_total = lax.psum_scatter(
        jnp.dot(dense_hidden, dense_down, preferred_element_type=jnp.float32) * mix_factor[:, None]
        + weight[:, None] * jnp.take(expert_out, slot_clip, axis=0),
        ("ep", "tp"),
        scatter_dimension=0,
        tiled=True,
    )
    layer_out = (resid + moe_total).astype(jnp.bfloat16)
    return (layer_out, new_state)


def solution(mesh):
    placed = (
        P(("ep", "tp"), None),
        P(),
        P(None, "tp", "ep"),
        P(None, "tp", "ep"),
        P(None, "tp", "ep"),
        P(None, "tp", "ep"),
        P(None, "tp"),
        P(None, "tp"),
        P("tp"),
        P("tp"),
        P(),
        P("ep", "tp", None, None),
        P("tp", "ep"),
        P(),
        P(),
        P(None, ("ep", "tp")),
        P(None, ("ep", "tp")),
        P(("ep", "tp"), None),
        P("ep", None, "tp"),
        P("ep", None, "tp"),
        P("ep", "tp", None),
        P(),
        P(),
    )
    return jax.shard_map(
        body,
        mesh=mesh,
        in_specs=placed,
        out_specs=(P(("ep", "tp"), None), P("ep", "tp", None, None)),
        check_vma=False,
    )
```

profile of v0, /device:TPU:0, one launch (start us, length us, event | category | flops | bytes accessed | tf_op | source)
XLA Modules:
  0.0 411.6 jit_solution(2718276647418501136)
XLA Ops:
  7.2 1.0 fusion.31
  8.3 1.5 fusion.33
  9.8 0.7 neg.38
  10.4 1.3 pad_maximum_fusion
  11.7 56.1 %all-gather.3.cloned.1.call-done = bf16[256,2048]{1,0:T(8,128)(2,1)} async-done(((bf16[8,2048]{1,0:T(8,128)(2,1)}), bf16[256,2048]{1,0:T(8,128)(2,1)}) %all-gather.3.cloned.1.call-update) | async-done | bytes 1048592 | tf_op jit(solution)/shard_map/all_gather | solution.py:51
  67.8 1.7 convolution_convert_fusion
  69.5 3.7 copy.52
  73.2 4.0 reshape.258
  77.2 4.6 %all-to-all-start = ((bf16[16,2,2048]{2,1,0:T(2,128)(2,1)}), bf16[16,2,2048]{2,1,0:T(2,128)(2,1)S(1)}, u32[]{:S(2)}, u32[]{:S(2)}) async-start(bf16[16,2,2048]{2,1,0:T(2,128)(2,1)} %reshape.258), calls=%async_computation | async-start | bytes 262144 | tf_op jit(solution)/shard_map/all_to_all | solution.py:62
  81.9 1.0 fusion.18
  83.0 1.0 fusion.53
  84.0 5.6 %all-to-all-done = bf16[16,2,2048]{2,1,0:T(2,128)(2,1)S(1)} async-done(((bf16[16,2,2048]{2,1,0:T(2,128)(2,1)}), bf16[16,2,2048]{2,1,0:T(2,128)(2,1)S(1)}, u32[]{:S(2)}, u32[]{:S(2)}) %all-to-all-start) | async-done | bytes 131104 | tf_op jit(solution)/shard_map/all_to_all | solution.py:62
  89.7 3.4 reshape.259
  93.1 2.7 copy.53
  95.8 1.9 reshape.231
  97.7 2.5 copy.73
  100.2 1.1 fusion.70
  101.3 1.2 copy.66
  102.5 0.1 multiply_reduce_fusion.3
  102.7 1.2 copy.67
  103.9 0.2 copy.68
  104.1 0.1 multiply_reduce_fusion.2
  104.3 0.1 broadcast_multiply_fusion.1
  104.4 9.4 %fusion.71 = f32[16,8,1,128]{3,2,1,0:T(1,128)S(1)} fusion(f32[16,8,128,1]{2,3,1,0:T(1,128)S(1)} %bitcast.153, f32[16,8,128,128]{3,2,1,0:T(8,128)} %param.34), kind=kOutput, calls=%fused_computation.123 | convolution fusion | flops 25165824 | bytes 8519680 | tf_op jit(solution)/shard_map/shkv,shk->shv/dot_general | solution.py:74
  113.9 5.7 %multiply_add_fusion = f32[16,8,128,128]{3,2,1,0:T(8,128)S(1)} fusion(f32[16,8,128,128]{3,2,1,0:T(8,128)} %param.34, f32[16,8,128]{2,1,0:T(8,128)S(1)} %fusion.44, f32[16,8,128]{2,1,0:T(8,128)S(1)} %get-tuple-element.6, f32[16,8]{1,0:T(8,128)S(1)} %copy.50), kind=kLoop, calls=%fused_computation.2 | loop fusion | flops 6291456 | bytes 16908800 | tf_op jit(solution)/shard_map/add | solution.py:77
  119.6 7.2 %fusion.72 = f32[16,8,1,128]{3,2,1,0:T(1,128)S(1)} fusion(f32[16,8,128,128]{3,2,1,0:T(8,128)S(1)} %multiply_add_fusion, f32[16,8,128,1]{2,3,1,0:T(1,128)S(1)} %bitcast.152), kind=kOutput, calls=%fused_computation.124 | convolution fusion | flops 25165824 | bytes 8519680 | tf_op jit(solution)/shard_map/shkv,shk->shv/dot_general | solution.py:80
  126.9 0.2 copy.69
  127.2 40.5 %all_gather.10 = bf16[256,1024]{1,0:T(8,128)(2,1)S(1)} all-gather(bf16[16,1024]{1,0:T(8,128)(2,1)S(1)} %bitcast.159), channel_id=1, replica_groups=mesh['ep'=16,'tp'=2] {'ep'}, dimensions={0}, use_global_device_ids=true | all-gather | bytes 557056 | tf_op jit(solution)/shard_map/all_gather | solution.py:84
  167.7 0.9 convolution_convert_fusion.1
  168.7 0.6 dynamic-slice
  169.3 13.1 %all-reduce.3.cloned.1.call-done = bf16[16,2,8,128]{3,2,1,0:T(8,128)(2,1)} async-done(((bf16[16,2,8,128]{3,2,1,0:T(8,128)(2,1)}), bf16[16,2,8,128]{3,2,1,0:T(8,128)(2,1)}) %all-reduce.3.cloned.1.call-update) | async-done | bytes 65552
  182.4 1.4 constant_dynamic-slice_fusion
  183.8 14.0 %all_to_all.8 = bf16[16,1,8,128]{3,2,1,0:T(8,128)(2,1)S(1)} all-to-all(bf16[16,1,8,128]{3,2,1,0:T(8,128)(2,1)S(1)} %constant_dynamic-slice_fusion), channel_id=1, replica_groups=mesh['ep'=16,'tp'=2] {'ep'}, dimensions={0} | all-to-all | bytes 65536 | tf_op jit(solution)/shard_map/all_to_all | solution.py:91
  197.8 0.1 multiply_reduce_fusion
  198.0 0.7 multiply_convert_fusion
  198.7 0.3 reduce-scatter.3.cloned.1.call-start
  199.1 0.2 reduce_window_sum.11
  199.5 0.1 select_reduce_fusion
  199.7 49.3 %all-gather.5.cloned.1.call-done = bf16[256,2048]{1,0:T(8,128)(2,1)} async-done(((bf16[8,2048]{1,0:T(8,128)(2,1)}), bf16[256,2048]{1,0:T(8,128)(2,1)}) %all-gather.5.cloned.1.call-update) | async-done | bytes 1048592 | tf_op jit(solution)/shard_map/all_gather | solution.py:99
  249.0 1.7 fusion.74
  250.7 1.7 gather_fusion
  252.4 2.2 fusion.5
  254.7 2.6 fusion.1
  257.3 2.7 gather_fusion.1
  260.0 1.9 fusion.73
  261.9 4.1 fusion
  266.0 137.6 %reduce-scatter.3.cloned.1.call-done = f32[8,2048]{1,0:T(8,128)} async-done(((f32[256,2048]{1,0:T(8,128)}), f32[8,2048]{1,0:T(8,128)}) %reduce-scatter.3.cloned.1.call-update) | async-done | bytes 65552 | tf_op jit(solution)/shard_map/reduce_scatter | solution.py:127
  403.6 1.5 add_convert_fusion
  (63 shorter events, 1.2 us)
Async XLA Ops:
  7.2 247.5 %copy-start = (bf16[1,512,2048]{2,1,0:T(8,128)(2,1)S(1)}, bf16[1,512,2048]{2,1,0:T(8,128)(2,1)}, u32[]{:S(2)}) copy-start(bf16[1,512,2048]{2,1,0:T(8,128)(2,1)} %param.43) | copy-start | bytes 6291460
  7.2 60.6 %all-gather.3.cloned.1.call-start = ((), (), s32[]{:S(2)}) async-start(), calls=%async_computation.3 | async-start | bytes 1081344 | tf_op jit(solution)/shard_map/all_gather | solution.py:51
  69.5 12.4 %copy-start.6 = (bf16[2048,8]{0,1:T(8,128)(2,1)S(1)}, bf16[2048,8]{0,1:T(8,128)(2,1)}, u32[]{:S(2)}) copy-start(bf16[2048,8]{0,1:T(8,128)(2,1)} %param.29) | copy-start | bytes 98308
  69.5 13.4 %copy-start.12 = (bf16[2048,8]{0,1:T(8,128)(2,1)S(1)}, bf16[2048,8]{0,1:T(8,128)(2,1)}, u32[]{:S(2)}) copy-start(bf16[2048,8]{0,1:T(8,128)(2,1)} %param.30) | copy-start | bytes 98308
  69.5 13.4 %copy-start.13 = (f32[8]{0:T(128)S(1)}, f32[8]{0:T(128)}, u32[]{:S(2)}) copy-start(f32[8]{0:T(128)} %param.32) | copy-start | bytes 100
  77.2 12.4 %all-to-all-start = ((bf16[16,2,2048]{2,1,0:T(2,128)(2,1)}), bf16[16,2,2048]{2,1,0:T(2,128)(2,1)S(1)}, u32[]{:S(2)}, u32[]{:S(2)}) async-start(bf16[16,2,2048]{2,1,0:T(2,128)(2,1)} %reshape.258), calls=%async_computation | async-start | bytes 262144 | tf_op jit(solution)/shard_map/all_to_all | solution.py:62
  81.8 100.5 %all-reduce.3.cloned.1.call-start = ((), (), s32[]{:S(2)}) async-start(), calls=%async_computation.6 | async-start | bytes 131072
  119.5 7.2 %copy-start.3 = (f32[16,8,128,128]{3,2,1,0:T(8,128)}, f32[16,8,128,128]{3,2,1,0:T(8,128)S(1)}, u32[]{:S(2)}) copy-start(f32[16,8,128,128]{3,2,1,0:T(8,128)S(1)} %multiply_add_fusion) | copy-start | bytes 25165828
  119.6 7.6 %copy-start.11 = (f32[128]{0:T(128)S(1)}, f32[128]{0:T(128)}, u32[]{:S(2)}) copy-start(f32[128]{0:T(128)} %param.33) | copy-start | bytes 1540
  119.6 48.1 %copy-start.5 = (bf16[1024,128]{1,0:T(8,128)(2,1)S(1)}, bf16[1024,128]{1,0:T(8,128)(2,1)}, u32[]{:S(2)}) copy-start(bf16[1024,128]{1,0:T(8,128)(2,1)} %param.35) | copy-start | bytes 786436
  126.8 41.9 %copy-start.14 = (u32[32]{0:T(128)S(1)}, u32[32]{0:T(128)}, u32[]{:S(2)}) copy-start(u32[32]{0:T(128)} %constant.108) | copy-start | bytes 388
  126.8 71.0 %copy-start.4 = (bf16[8,2048]{1,0:T(8,128)(2,1)S(1)}, bf16[8,2048]{1,0:T(8,128)(2,1)}, u32[]{:S(2)}) copy-start(bf16[8,2048]{1,0:T(8,128)(2,1)} %param.23) | copy-start | bytes 98308
  126.8 71.2 %copy-start.7 = (f32[2048]{0:T(1024)S(1)}, f32[2048]{0:T(1024)}, u32[]{:S(2)}) copy-start(f32[2048]{0:T(1024)} %param.36) | copy-start | bytes 24580
  126.8 72.2 %copy-start.9 = (f32[256,4]{0,1:T(4,128)S(1)}, f32[256,4]{0,1:T(4,128)}, u32[]{:S(2)}) copy-start(f32[256,4]{0,1:T(4,128)} %param.45) | copy-start | bytes 12292
  126.8 72.2 %copy-start.10 = (s32[256,4]{0,1:T(4,128)S(1)}, s32[256,4]{0,1:T(4,128)}, u32[]{:S(2)}) copy-start(s32[256,4]{0,1:T(4,128)} %param.44) | copy-start | bytes 12292
  126.8 72.6 %copy-start.8 = (bf16[2048]{0:T(1024)(128)(2,1)S(1)}, bf16[2048]{0:T(1024)(128)(2,1)}, u32[]{:S(2)}) copy-start(bf16[2048]{0:T(1024)(128)(2,1)} %param.37) | copy-start | bytes 12292
  168.6 80.3 %all-gather.5.cloned.1.call-start = ((), (), s32[]{:S(2)}) async-start(), calls=%async_computation.4 | async-start | bytes 1081344 | tf_op jit(solution)/shard_map/all_gather | solution.py:99
  198.7 204.9 %reduce-scatter.3.cloned.1.call-start = ((), (), s32[]{:S(2)}) async-start(), calls=%async_computation.5 | async-start | bytes 2162688 | tf_op jit(solution)/shard_map/reduce_scatter | solution.py:127
  249.0 1.7 copy-start.1
  260.0 1.9 copy-start.2
Sparse Core Ops, SparseCore 0:
  11.4 56.3 all-gather.2
  168.8 13.5 all-reduce.2
  198.8 50.1 all-gather.4
  266.1 137.4 reduce-scatter.2
where the time goes:
time: 413 us; the launch traced here: 412 us
  waiting for transfers between devices  262 us (63%)
  blocking collectives  54.5 us (13%)
  matrix products  33.7 us (8%)
  local copies, waits for them, and re-layouts  29.1 us (7%)
  between operations  14.1 us (3%)
  other arithmetic  13.5 us (3%)
  starting transfers between devices  4.98 us (1%)
    reduce_scatter x1, waiting for transfers between devices, body(): lax.psum_scatter(jnp.dot(dense_hidden, dense_down, preferred_element_type...  138 us
    all_gather x1, waiting for transfers between devices, body(): rows_all = lax.all_gather(normed, ('ep', 'tp'), axis=0, tiled=True)  56.1 us
    all_gather x1, waiting for transfers between devices, body(): moe_all = lax.all_gather(moe_in, ('ep', 'tp'), axis=0, tiled=True)  49.3 us
    all_gather x1, blocking collectives, body(): lax.all_gather(gated, 'ep', axis=0, tiled=True)  40.5 us
    all_to_all x1, blocking collectives, body(): lax.all_to_all(partial_value.astype(jnp.bfloat16), 'ep', split_axis=0, co...  14 us
    unnamed x5, waiting for transfers between devices  13.2 us
    unnamed x40, local copies, waits for them, and re-layouts  12.4 us
    dot_general x1, matrix products, body(): jnp.einsum('shkv,shk->shv', state, key_vec, precision=lax.Precision.HIGHEST)  9.38 us
  transfers between devices with their start and end apart: 5, of which 5 were waited for; matrix products, arithmetic and copies ran while one was open for 1% of the time, Pallas kernels for 0%

commit v1 on v0

v1 whole, which is shorter than its diff:
```python
import functools

import jax
import jax.numpy as jnp
from jax import lax
from jax.experimental import pallas as pl
from jax.experimental.pallas import tpu as pltpu
from jax.sharding import PartitionSpec as P

EPS = 1e-06
VMEM = pltpu.VMEM
MESH = pl.DeviceIdType.MESH


def rms_scale(values, gain):
    return values * lax.rsqrt(jnp.mean(values * values, axis=-1, keepdims=True) + EPS) * gain


def grid_of(count):
    for depth in (4, 2, 1):
        side = int(round((count / depth) ** 0.5))
        if depth * side * side == count:
            return depth, side
    return count, 1


def place(count):
    depth, side = grid_of(count)
    ep = lax.axis_index("ep")
    t = lax.axis_index("tp")
    z = ep // (side * side)
    y = (ep // side) % side
    x = ep % side
    a = x * (1 - t) + y * t
    b = y * (1 - t) + x * t
    return depth, side, t, z, b, a


def ep_of(side, t, z, b, a):
    y = b * (1 - t) + a * t
    x = a * (1 - t) + b * t
    return (z * side + y) * side + x


def greet(devices):
    barrier = pltpu.get_barrier_semaphore()
    for device in devices:
        pl.semaphore_signal(barrier, inc=1, device_id=device, device_id_type=MESH)
    pl.semaphore_wait(barrier, len(devices))


def gather_kernel(count, both, block_ref, out_ref, send_sem, recv_sem):
    depth, side, t, z, b, a = place(count)
    zs = [((lax.rem(z + i, depth)), b, a) for i in range(1, depth)]
    bs = [(z, lax.rem(b + i, side), a) for i in range(1, side)]
    as_ = [(z, b, lax.rem(a + i, side)) for i in range(1, side)]
    device_of = lambda c: (ep_of(side, t, *c), t)
    peers = [device_of(c) for c in zs + bs + as_]
    partner = (lax.axis_index("ep"), 1 - t)
    greet(peers + ([partner] if both else []))
    width = 2 if both else 1
    slot_of = lambda dz, db, da: (
        ep_of(side, t, lax.rem(z + dz, depth), lax.rem(b + db, side), lax.rem(a + da, side)) * width
        + (t if both else 0)
    )
    mine = slot_of(0, 0, 0)
    out_ref[mine] = block_ref[...]
    counter = [0]
    started = []
    arrivals = {}

    def send(src, offset, key, device):
        number = counter[0]
        counter[0] += 1
        copy = pltpu.make_async_remote_copy(
            src_ref=src,
            dst_ref=out_ref.at[slot_of(*offset)],
            send_sem=send_sem.at[number],
            recv_sem=recv_sem.at[number],
            device_id=device,
            device_id_type=MESH,
        )
        copy.start()
        started.append(copy)
        arrivals[key] = copy

    def relay(offset, legs):
        dz, db, da = offset
        src = block_ref if offset == (0, 0, 0) else out_ref.at[slot_of(*offset)]
        if "a" in legs:
            for i in range(1, side):
                send(src, offset, ("a", (dz, db, (da - i) % side)), device_of(as_[i - 1]))
        if "b" in legs:
            for i in range(1, side):
                send(src, offset, ("b", (dz, (db - i) % side, da)), device_of(bs[i - 1]))
        if "z" in legs:
            for i in range(1, depth):
                send(src, offset, ("z", ((dz - i) % depth, db, da)), device_of(zs[i - 1]))
        if both:
            send(src, offset, ("t", offset), partner)

    relay((0, 0, 0), "zba")
    for dz in range(1, depth):
        arrivals["z", (dz, 0, 0)].wait_recv()
        relay((dz, 0, 0), "ba")
    for dz in range(depth):
        for db in range(1, side):
            arrivals["b", (dz, db, 0)].wait_recv()
            relay((dz, db, 0), "a")
    for dz in range(depth):
        for db in range(side):
            for da in range(1, side):
                arrivals["a", (dz, db, da)].wait_recv()
                relay((dz, db, da), "")
    if both:
        for key, copy in arrivals.items():
            if key[0] == "t":
                copy.wait_recv()
    for copy in started:
        copy.wait_send()


def gather(block, count, both, number):
    total = count * (2 if both else 1)
    depth, side = grid_of(count)
    copies = count - 1 + (count if both else 0)
    return pl.pallas_call(
        functools.partial(gather_kernel, count, both),
        out_shape=jax.ShapeDtypeStruct((total,) + block.shape, block.dtype),
        in_specs=[pl.BlockSpec(memory_space=VMEM)],
        out_specs=pl.BlockSpec(memory_space=VMEM),
        scratch_shapes=[
            pltpu.SemaphoreType.DMA((copies,)),
            pltpu.SemaphoreType.DMA((copies,)),
        ],
        compiler_params=pltpu.CompilerParams(collective_id=number, has_side_effects=True),
        name=f"gather_{number}",
    )(block)


def exchange_kernel(count, both, blocks_ref, out_ref, send_sem, recv_sem):
    ep = lax.axis_index("ep")
    t = lax.axis_index("tp")
    total = count * 2 if both else count
    me = ep * 2 + t if both else ep

    def device(i):
        other = lax.rem(me + i, total)
        return other, ((other // 2, other % 2) if both else (other, t))

    barrier = pltpu.get_barrier_semaphore()

    def hello(i, carry):
        pl.semaphore_signal(barrier, inc=1, device_id=device(i)[1], device_id_type=MESH)
        return carry

    lax.fori_loop(1, total, hello, 0)
    pl.semaphore_wait(barrier, total - 1)

    def copy(i):
        other, target = device(i)
        return pltpu.make_async_remote_copy(
            src_ref=blocks_ref.at[other],
            dst_ref=out_ref.at[me],
            send_sem=send_sem.at[i],
            recv_sem=recv_sem.at[i],
            device_id=target,
            device_id_type=MESH,
        )

    def start(i, carry):
        copy(i).start()
        return carry

    def finish(i, carry):
        copy(i).wait()
        return carry

    lax.fori_loop(1, total, start, 0)
    out_ref[me] = blocks_ref[me]
    lax.fori_loop(1, total, finish, 0)


def exchange(blocks, count, both, number):
    return pl.pallas_call(
        functools.partial(exchange_kernel, count, both),
        out_shape=jax.ShapeDtypeStruct(blocks.shape, blocks.dtype),
        in_specs=[pl.BlockSpec(memory_space=VMEM)],
        out_specs=pl.BlockSpec(memory_space=VMEM),
        scratch_shapes=[
            pltpu.SemaphoreType.DMA((blocks.shape[0],)),
            pltpu.SemaphoreType.DMA((blocks.shape[0],)),
        ],
        compiler_params=pltpu.CompilerParams(collective_id=number, has_side_effects=True),
        name=f"exchange_{number}",
    )(blocks)


def scatter_kernel(
    count, part_ref, out_ref, core_buf, sum1, a_buf, sum2, b_buf, sum3, z_buf, send_sem, recv_sem
):
    depth, side, t, z, b, a = place(count)
    device_of = lambda dz, db, da: (
        ep_of(side, t, lax.rem(z + dz, depth), lax.rem(b + db, side), lax.rem(a + da, side)),
        t,
    )
    partner = (lax.axis_index("ep"), 1 - t)
    greet(
        [partner]
        + [device_of(i, 0, 0) for i in range(1, depth)]
        + [device_of(0, i, 0) for i in range(1, side)]
        + [device_of(0, 0, i) for i in range(1, side)]
    )
    flat = lambda core, dz, db, da: (
        ep_of(side, t, lax.rem(z + dz, depth), lax.rem(b + db, side), lax.rem(a + da, side)) * 2
        + core
    )
    counter = [0]
    started = []

    def send(src, dst, device, number=None):
        if number is None:
            number = count + counter[0]
            counter[0] += 1
        copy = pltpu.make_async_remote_copy(
            src_ref=src,
            dst_ref=dst,
            send_sem=send_sem.at[number],
            recv_sem=recv_sem.at[number],
            device_id=device,
            device_id_type=MESH,
        )
        copy.start()
        started.append(copy)
        return copy

    add = lambda first, *rest: functools.reduce(
        lambda u, v: u + v, [w.astype(jnp.float32) for w in (first,) + rest]
    )
    order = [
        (dz, db, da)
        for da in list(range(1, side)) + [0]
        for db in list(range(1, side)) + [0]
        for dz in list(range(1, depth)) + [0]
    ]
    absolute = lambda dz, db, da: ep_of(
        side, t, lax.rem(z + dz, depth), lax.rem(b + db, side), lax.rem(a + da, side)
    )
    for dz, db, da in order:
        spot = absolute(dz, da, db)
        send(part_ref.at[spot * 2 + 1 - t], core_buf.at[spot], partner, spot)

    def core_arrival(spot):
        return pltpu.make_async_remote_copy(
            src_ref=part_ref.at[spot * 2 + 1 - t],
            dst_ref=core_buf.at[spot],
            send_sem=send_sem.at[spot],
            recv_sem=recv_sem.at[spot],
            device_id=partner,
            device_id_type=MESH,
        )

    a_copies = {}
    for c in order:
        dz, db, da = c
        core_arrival(absolute(*c)).wait_recv()
        total = add(part_ref[absolute(*c) * 2 + t], core_buf[absolute(*c)])
        slot = (da * side + db) * depth + dz
        sum1[slot] = total.astype(sum1.dtype)
        if da:
            a_copies[c] = send(
                sum1.at[slot], a_buf.at[(da * side + db) * depth + dz], device_of(0, 0, da)
            )
    b_copies = {}
    for db in list(range(1, side)) + [0]:
        for dz in list(range(1, depth)) + [0]:
            terms = [sum1[db * depth + dz]]
            for da in range(1, side):
                a_copies[dz, db, da].wait_recv()
                terms.append(a_buf[(da * side + db) * depth + dz])
            sum2[db * depth + dz] = add(*terms).astype(sum2.dtype)
            if db:
                b_copies[dz, db] = send(
                    sum2.at[db * depth + dz], b_buf.at[db * depth + dz], device_of(0, db, 0)
                )
    z_copies = []
    for dz in list(range(1, depth)) + [0]:
        terms = [sum2[dz]]
        for db in range(1, side):
            b_copies[dz, db].wait_recv()
            terms.append(b_buf[db * depth + dz])
        total = add(*terms)
        if dz:
            sum3[dz] = total.astype(sum3.dtype)
            z_copies.append(send(sum3.at[dz], z_buf.at[dz], device_of(dz, 0, 0)))
    for dz in range(1, depth):
        z_copies[dz - 1].wait_recv()
        total = total + z_buf[dz].astype(jnp.float32)
    out_ref[...] = total
    for copy in started:
        copy.wait_send()


def scatter(parts, count, number):
    depth, side = grid_of(count)
    block = parts.shape[1:]
    copies = count + (side - 1) * side * depth + (side - 1) * depth + depth - 1
    buf = lambda n: pltpu.VMEM((n,) + block, parts.dtype)
    return pl.pallas_call(
        functools.partial(scatter_kernel, count),
        out_shape=jax.ShapeDtypeStruct(block, jnp.float32),
        in_specs=[pl.BlockSpec(memory_space=VMEM)],
        out_specs=pl.BlockSpec(memory_space=VMEM),
        scratch_shapes=[
            buf(count),
            buf(count),
            buf(count),
            buf(side * depth),
            buf(side * depth),
            buf(depth),
            buf(depth),
            pltpu.SemaphoreType.DMA((copies,)),
            pltpu.SemaphoreType.DMA((copies,)),
        ],
        compiler_params=pltpu.CompilerParams(collective_id=number, has_side_effects=True),
        name=f"scatter_{number}",
    )(parts)


def delta_kernel(heads, rows_ref, cols_ref, retain_ref, beta_ref, gain_ref, state_ref, gated_ref, new_ref):
    head_size = cols_ref.shape[1]
    silu = lambda v: v / (1.0 + jnp.exp(-v))
    cols = silu(cols_ref[0])
    cols = cols * lax.rsqrt(jnp.sum(cols * cols, axis=0, keepdims=True) + EPS)
    rows = silu(rows_ref[0])
    value, gate = rows[:heads], rows[heads:]
    readouts = []
    for h in range(heads):
        query = cols[:, h : h + 1] * head_size ** (-0.5)
        key = cols[:, heads + h : heads + h + 1]
        keep = retain_ref[0, h : h + 1, :]
        old = state_ref[0, h]
        recalled = jnp.sum(old * key, axis=0, keepdims=True)
        correction = value[h : h + 1] - keep * recalled
        new = keep * old + key * (beta_ref[0, h : h + 1, :] * correction)
        new_ref[0, h] = new
        readouts.append(jnp.sum(new * query, axis=0, keepdims=True))
    readout = jnp.concatenate(readouts, axis=0)
    gated = rms_scale(readout, gain_ref[...]) * gate
    gated_ref[0] = gated.astype(gated_ref.dtype)


def delta(rows, cols, retain, beta, gain, state):
    seqs, heads, size, _ = state.shape
    own = lambda *shape: pl.BlockSpec((1,) + shape, lambda s: (s,) + (0,) * len(shape))
    return pl.pallas_call(
        functools.partial(delta_kernel, heads),
        grid=(seqs,),
        out_shape=(
            jax.ShapeDtypeStruct((seqs, heads, size), jnp.bfloat16),
            jax.ShapeDtypeStruct(state.shape, state.dtype),
        ),
        in_specs=[
            own(2 * heads, size),
            own(size, 2 * heads),
            own(heads, size),
            own(heads, size),
            pl.BlockSpec((1, size), lambda s: (0, 0)),
            own(heads, size, size),
        ],
        out_specs=(own(heads, size), own(heads, size, size)),
        compiler_params=pltpu.CompilerParams(dimension_semantics=("arbitrary",)),
        name="delta",
    )(rows, cols, retain, beta, gain.reshape(1, size), state)


def body(
    tokens,
    mix_gain,
    w_query,
    w_key,
    w_value,
    w_zgate,
    w_beta,
    w_decay,
    decay_rate,
    decay_bias,
    head_gain,
    state,
    w_out,
    moe_gain,
    dense_mix,
    dense_gate,
    dense_up,
    dense_down,
    expert_gate,
    expert_up,
    expert_down,
    expert_ids,
    route_weight,
):
    ep_count = lax.axis_size("ep")
    group_idx = lax.axis_index("ep")
    own_rows, width = tokens.shape
    seqs, heads, size, _ = state.shape
    part = w_query.shape[2]
    total_rows = ep_count * seqs
    tok_float = tokens.astype(jnp.float32)
    normed = rms_scale(tok_float, mix_gain).astype(jnp.bfloat16)
    rows_all = gather(normed, ep_count, True, 1).reshape(total_rows, width)
    w_cat = jnp.stack([w_query, w_key, w_value, w_zgate], axis=1).reshape(width, -1)
    projected = jnp.dot(rows_all, w_cat, preferred_element_type=jnp.float32)
    projected = projected.astype(jnp.bfloat16).reshape(ep_count, seqs, -1)
    swapped = exchange(projected, ep_count, False, 2)
    swapped = swapped.reshape(ep_count, seqs, 2, 2 * heads, part).astype(jnp.float32)
    cols = swapped[:, :, 0].transpose(1, 0, 3, 2).reshape(seqs, size, 2 * heads)
    rows = swapped[:, :, 1].transpose(1, 2, 0, 3).reshape(seqs, 2 * heads, size)
    seq_rows = lax.dynamic_slice_in_dim(rows_all, group_idx * seqs, seqs, 0)
    rates = jnp.dot(
        seq_rows, jnp.concatenate([w_beta, w_decay], axis=1), preferred_element_type=jnp.float32
    )
    beta_rate = jax.nn.sigmoid(rates[:, :heads])
    retain = jnp.exp(-decay_rate * jax.nn.softplus(rates[:, heads:] + decay_bias))
    spread = lambda v: jnp.broadcast_to(v[:, :, None], (seqs, heads, size))
    gated, new_state = delta(rows, cols, spread(retain), spread(beta_rate), head_gain, state)
    gated_all = gather(gated.reshape(seqs, heads * size), ep_count, False, 3)
    partial_value = jnp.dot(
        gated_all.reshape(total_rows, heads * size), w_out, preferred_element_type=jnp.float32
    )
    partial_value = partial_value.astype(jnp.bfloat16).reshape(-1, own_rows, w_out.shape[1])
    mixed = exchange(partial_value, ep_count, True, 4).astype(jnp.float32)
    mixed = mixed.reshape(ep_count, -1, own_rows, w_out.shape[1]).sum(axis=1)
    resid = tok_float + mixed.transpose(1, 0, 2).reshape(own_rows, width)
    moe_in = rms_scale(resid, moe_gain).astype(jnp.bfloat16)
    moe_all = gather(moe_in, ep_count, True, 5).reshape(total_rows, width)

    def branch(gate, up, down):
        hidden = jax.nn.silu(jnp.dot(moe_all, gate, preferred_element_type=jnp.float32))
        hidden = hidden * jnp.dot(moe_all, up, preferred_element_type=jnp.float32)
        return jnp.dot(hidden.astype(jnp.bfloat16), down, preferred_element_type=jnp.float32)

    mix_factor = jax.nn.sigmoid(jnp.dot(moe_all, dense_mix, preferred_element_type=jnp.float32))
    weight = jnp.sum(jnp.where(expert_ids == group_idx, route_weight, 0.0), axis=1)
    terms = mix_factor[:, None] * branch(dense_gate, dense_up, dense_down)
    terms = terms + weight[:, None] * branch(expert_gate[0], expert_up[0], expert_down[0])
    terms = terms.astype(jnp.bfloat16).reshape(-1, own_rows, width)
    layer_out = (resid + scatter(terms, ep_count, 6)).astype(jnp.bfloat16)
    return (layer_out, new_state)


def solution(mesh):
    placed = (
        P(("ep", "tp"), None),
        P(),
        P(None, "tp", "ep"),
        P(None, "tp", "ep"),
        P(None, "tp", "ep"),
        P(None, "tp", "ep"),
        P(None, "tp"),
        P(None, "tp"),
        P("tp"),
        P("tp"),
        P(),
        P("ep", "tp", None, None),
        P("tp", "ep"),
        P(),
        P(),
        P(None, ("ep", "tp")),
        P(None, ("ep", "tp")),
        P(("ep", "tp"), None),
        P("ep", None, "tp"),
        P("ep", None, "tp"),
        P("ep", "tp", None),
        P(),
        P(),
    )
    return jax.shard_map(
        body,
        mesh=mesh,
        in_specs=placed,
        out_specs=(P(("ep", "tp"), None), P("ep", "tp", None, None)),
        check_vma=False,
    )
```

time: 413 us -> 147 us (0.36)
  waiting for transfers between devices: 262 us -> 0 us
  Pallas kernels: 0 us -> 103 us
  blocking collectives: 54.5 us -> 0 us
  local copies, waits for them, and re-layouts: 29.1 us -> 13.9 us
  matrix products: 33.7 us -> 18.8 us
  between operations: 14.1 us -> 0.79 us
  starting transfers between devices: 4.98 us -> 0 us
  other arithmetic: 13.5 us -> 9.1 us
    reduce_scatter x1 -> x0, waiting for transfers between devices: 138 us -> none  [body(): lax.psum_scatter(jnp.dot(dense_hidden, dense_down, preferred_element_type...]
    all_gather x2 -> x0, waiting for transfers between devices: 105 us -> none  [the longest x1 56.1 us: body(): rows_all = lax.all_gather(normed, ('ep', 'tp'), axis=0, tiled=True)]
    pallas_call x0 -> x7, Pallas kernels: none -> 103 us  [the longest x3 52 us: gather(): pl.pallas_call(functools.partial(gather_kernel, count, both), out_shape=j...]
    all_gather x1 -> x0, blocking collectives: 40.5 us -> none  [body(): lax.all_gather(gated, 'ep', axis=0, tiled=True)]
    dot_general x10 -> x7, matrix products: 32 us -> 17.1 us  [the longest x2 8.06 us: branch(): jnp.dot(hidden.astype(jnp.bfloat16), down, preferred_element_type=jnp.flo...]
    all_to_all x1 -> x0, blocking collectives: 14 us -> none  [body(): lax.all_to_all(partial_value.astype(jnp.bfloat16), 'ep', split_axis=0, co...]
    unnamed x5 -> x0, waiting for transfers between devices: 13.2 us -> none
    unnamed x40 -> x14, local copies, waits for them, and re-layouts: 12.4 us -> 2.09 us
  transfers between devices with their start and end apart: 5 -> 0, of which waited for: 5 -> 0; matrix products, arithmetic and copies ran while one was open for 1% -> 0% of each run, Pallas kernels for 0% -> 0%
where the time goes in v1:
time: 147 us; the launch traced here: 146 us
  Pallas kernels  103 us (70%)
  matrix products  18.8 us (13%)
  local copies, waits for them, and re-layouts  13.9 us (9%)
  other arithmetic  9.1 us (6%)
    pallas_call x3, Pallas kernels, gather(): pl.pallas_call(functools.partial(gather_kernel, count, both), out_shape=j...  52 us
    pallas_call x2, Pallas kernels, exchange(): pl.pallas_call(functools.partial(exchange_kernel, count, both), out_shape...  19.8 us
    pallas_call x1, Pallas kernels, scatter(): pl.pallas_call(functools.partial(scatter_kernel, count), out_shape=jax.Sh...  16.1 us
    pallas_call x1, Pallas kernels, delta(): pl.pallas_call(functools.partial(delta_kernel, heads), grid=(seqs,), out_...  15 us
    dot_general x2, matrix products, branch(): jnp.dot(hidden.astype(jnp.bfloat16), down, preferred_element_type=jnp.flo...  8.06 us
    dot_general x2, matrix products, branch(): jnp.dot(moe_all, gate, preferred_element_type=jnp.float32)  4.88 us
    transpose x2, local copies, waits for them, and re-layouts, body(): cols = swapped[:, :, 0].transpose(1, 0, 3, 2).reshape(seqs, size, 2 * heads)  4.59 us

profile of v1, /device:TPU:0, one launch (start us, length us, event | category | flops | bytes accessed | tf_op | source)
XLA Modules:
  0.0 145.6 jit_solution(5687439377201956036)
XLA Ops:
  0.6 0.0 copy-start
  0.7 0.8 neg.21
  1.5 0.7 select_reduce_fusion
  2.2 0.9 fusion.39
  3.1 0.7 reshape.90
  3.8 1.4 fusion.41.block_ref
  5.2 19.6 %gather_1.1 = bf16[32,8,2048]{2,1,0:T(8,128)(2,1)} custom-call(bf16[8,2048]{1,0:T(8,128)(2,1)} %fusion.41.block_ref), custom_call_target="tpu_custom_call" | custom-call | tf_op jit(solution)/shard_map/gather_1/pallas_call | solution.py:127
  24.9 0.0 copy-start.2
  24.9 1.1 fusion.42
  26.0 0.7 fusion.52
  26.7 0.1 copy.33
  26.8 0.1 copy.32
  26.9 0.7 broadcast_in_dim.7.retain_ref
  27.6 0.7 broadcast_in_dim.8.beta_ref
  28.3 1.3 pad_maximum_fusion
  29.6 0.0 copy-done.2
  29.6 1.1 convolution_convert_fusion
  30.7 9.8 %exchange_2.1 = bf16[16,16,256]{2,1,0:T(8,128)(2,1)} custom-call(bf16[16,16,256]{2,1,0:T(8,128)(2,1)} %bitcast.86), custom_call_target="tpu_custom_call" | custom-call | tf_op jit(solution)/shard_map/exchange_2/pallas_call | solution.py:185
  40.6 2.6 %copy.29 = f32[16,16,256]{1,2,0:T(8,128)} copy(bf16[16,16,256]{2,1,0:T(8,128)(2,1)} %exchange_2.1) | data formatting | bytes 393216 | tf_op jit(solution)/shard_map/convert_element_type | solution.py:415
  43.2 2.8 %slice_bitcast_fusion = (f32[16,16,8,16]{0,2,3,1:T(8,128)S(1)}, f32[16,16,16,8]{0,3,1,2:T(8,128)}) fusion(f32[16,16,2,16,8]{1,4,3,2,0:T(8,128)} %bitcast.80), kind=kLoop, calls=%fused_computation.17 | loop fusion | bytes 524288 | tf_op jit(solution)/shard_map/transpose | solution.py:416
  45.9 1.8 %copy.31 = f32[16,16,8,16]{3,2,1,0:T(8,128)} copy(f32[16,16,8,16]{0,2,3,1:T(8,128)S(1)} %get-tuple-element.6) | data formatting | bytes 262144 | tf_op jit(solution)/shard_map/transpose | solution.py:416
  47.8 2.1 %copy.30 = f32[16,16,16,8]{1,3,2,0:T(8,128)S(1)} copy(f32[16,16,16,8]{0,3,1,2:T(8,128)} %get-tuple-element.7) | data formatting | bytes 262144 | tf_op jit(solution)/shard_map/transpose | solution.py:417
  49.9 1.0 copy.34.rows_ref
  50.8 0.0 copy-start.4
  50.8 0.0 copy-start.3
  50.8 0.0 copy-start.5
  50.8 15.0 %delta.1 = (bf16[16,8,128]{2,1,0:T(8,128)(2,1)}, f32[16,8,128,128]{3,2,1,0:T(8,128)}) custom-call(f32[16,16,128]{2,1,0:T(8,128)} %copy.34.rows_ref, f32[16,128,16]{2,1,0:T(8,128)} %bitcast.81, f32[16,8,128]{2,1,0:T(8,128)} %broadcast_in_dim.7.retain_ref, f32[16,8,128]{2,1,0:T(8,128)} %broadcast_in_dim.8.beta_ref, f32[1,128]{1,0:T(1,128)} %bitcast.94, ...), custom_call_target="tpu_custom_call" | custom-call | tf_op jit(solution)/shard_map/delta/pallas_call | solution.py:356
  65.9 1.4 copy.37
  67.2 15.2 %gather_3.1 = bf16[16,16,1024]{2,1,0:T(8,128)(2,1)} custom-call(bf16[16,1024]{1,0:T(8,128)(2,1)} %bitcast.91), custom_call_target="tpu_custom_call" | custom-call | tf_op jit(solution)/shard_map/gather_3/pallas_call | solution.py:127
  82.5 0.0 copy-done.4
  82.5 2.0 %fusion.15.blocks_ref = bf16[32,8,128]{2,1,0:T(8,128)(2,1)} fusion(bf16[256,1024]{1,0:T(8,128)(2,1)} %bitcast.85, bf16[1024,128]{1,0:T(8,128)(2,1)S(1)} %copy-done.4), kind=kOutput, calls=%fused_computation.16 | convolution fusion | flops 67141632 | bytes 851968 | tf_op jit(solution)/shard_map/dot_general | solution.py:427
  84.4 9.9 %exchange_4.1 = bf16[32,8,128]{2,1,0:T(8,128)(2,1)} custom-call(bf16[32,8,128]{2,1,0:T(8,128)(2,1)} %fusion.15.blocks_ref), custom_call_target="tpu_custom_call" | custom-call | tf_op jit(solution)/shard_map/exchange_4/pallas_call | solution.py:185
  94.4 0.9 convert_reduce_fusion
  95.2 0.0 copy-done.3
  95.3 0.1 multiply_reduce_fusion
  95.4 0.0 copy-done.5
  95.4 0.7 multiply_convert_fusion.block_ref
  96.1 17.2 %gather_5.1 = bf16[32,8,2048]{2,1,0:T(8,128)(2,1)} custom-call(bf16[8,2048]{1,0:T(8,128)(2,1)} %multiply_convert_fusion.block_ref), custom_call_target="tpu_custom_call" | custom-call | tf_op jit(solution)/shard_map/gather_5/pallas_call | solution.py:127
  113.3 0.0 copy-start.1
  113.3 1.7 %fusion.22 = f32[1,256]{1,0:T(1,128)S(1)} fusion(bf16[2048,1]{0,1:T(2,128)(2,1)S(1)} %reshape.90, bf16[32,8,2048]{2,1,0:T(8,128)(2,1)} %gather_5.1), kind=kOutput, calls=%fused_computation.25 | convolution fusion | flops 1048576 | bytes 1053696 | tf_op jit(solution)/shard_map/dot_general | solution.py:442
  115.0 1.8 %fusion.20 = f32[256,128]{1,0:T(8,128)S(1)} fusion(bf16[2048,128]{1,0:T(8,128)(2,1)} %param.38, bf16[32,8,2048]{2,1,0:T(8,128)(2,1)} %gather_5.1), kind=kOutput, calls=%fused_computation.23 | convolution fusion | flops 134217728 | bytes 1703936 | tf_op jit(solution)/shard_map/dot_general | solution.py:438
  116.8 0.0 copy-done.1
  116.8 3.1 %fusion.6 = f32[256,512]{1,0:T(8,128)} fusion(bf16[1,2048,512]{2,1,0:T(8,128)(2,1)} %param.41, bf16[32,8,2048]{2,1,0:T(8,128)(2,1)S(1)} %copy-done.1), kind=kOutput, calls=%fused_computation.8 | convolution fusion | flops 536870912 | bytes 3670016 | tf_op jit(solution)/shard_map/dot_general | solution.py:438
  119.9 3.3 %convolution_multiply_fusion.1 = f32[256,2048]{1,0:T(8,128)} fusion(bf16[128,2048]{1,0:T(8,128)(2,1)} %param.40, bf16[2048,128]{1,0:T(8,128)(2,1)} %param.39, bf16[32,8,2048]{2,1,0:T(8,128)(2,1)S(1)} %copy-done.1, f32[256]{0:T(256)S(1)} %add_divide_fusion, f32[256,128]{1,0:T(8,128)S(1)} %fusion.20), kind=kOutput, calls=%fused_computation.2 | convolution fusion | flops 269156352 | bytes 4326400 | tf_op jit(solution)/shard_map/dot_general | solution.py:440
  123.2 0.0 copy-done
  123.2 4.7 %fusion.2.part_ref = bf16[32,8,2048]{2,1,0:T(8,128)(2,1)} fusion(f32[256,2048]{1,0:T(8,128)} %convolution_multiply_fusion.1, bf16[1,512,2048]{2,1,0:T(8,128)(2,1)S(1)} %copy-done, f32[256]{0:T(256)S(1)} %select_reduce_fusion, bf16[1,2048,512]{2,1,0:T(8,128)(2,1)} %param.42, bf16[32,8,2048]{2,1,0:T(8,128)(2,1)S(1)} %copy-done.1, f32[256,512]{1,0:T(8,128)} %fusion.6), kind=kOutput, calls=%fused_computation.4 | convolution fusion | flops 1076101120 | bytes 8913920 | tf_op jit(solution)/shard_map/dot_general | solution.py:440
  127.9 16.1 %scatter_6.1 = f32[8,2048]{1,0:T(8,128)} custom-call(bf16[32,8,2048]{2,1,0:T(8,128)(2,1)} %fusion.2.part_ref), custom_call_target="tpu_custom_call" | custom-call | tf_op jit(solution)/shard_map/scatter_6/pallas_call | solution.py:309
  144.1 1.5 %add_convert_fusion = bf16[8,2048]{1,0:T(8,128)(2,1)} fusion(f32[8,2048]{1,0:T(8,128)} %scatter_6.1, f32[16,8,128]{2,1,0:T(8,128)S(1)} %convert_reduce_fusion, bf16[8,2048]{1,0:T(8,128)(2,1)S(1)} %copy-done.3), kind=kLoop, calls=%fused_computation.49 | loop fusion | flops 65536 | bytes 196608 | tf_op jit(solution)/shard_map/convert_element_type | solution.py:447
  (3 shorter events, 0.0 us)
Async XLA Ops:
  0.6 122.6 %copy-start = (bf16[1,512,2048]{2,1,0:T(8,128)(2,1)S(1)}, bf16[1,512,2048]{2,1,0:T(8,128)(2,1)}, u32[]{:S(2)}) copy-start(bf16[1,512,2048]{2,1,0:T(8,128)(2,1)} %param.43) | copy-start | bytes 6291460
  24.9 4.7 %copy-start.2 = (bf16[32,8,2048]{2,1,0:T(8,128)(2,1)S(1)}, bf16[32,8,2048]{2,1,0:T(8,128)(2,1)}, u32[]{:S(2)}) copy-start(bf16[32,8,2048]{2,1,0:T(8,128)(2,1)} %gather_1.1) | copy-start | bytes 3145732
  50.8 31.6 %copy-start.4 = (bf16[1024,128]{1,0:T(8,128)(2,1)S(1)}, bf16[1024,128]{1,0:T(8,128)(2,1)}, u32[]{:S(2)}) copy-start(bf16[1024,128]{1,0:T(8,128)(2,1)} %param.35) | copy-start | bytes 786436
  50.8 44.4 %copy-start.3 = (bf16[8,2048]{1,0:T(8,128)(2,1)S(1)}, bf16[8,2048]{1,0:T(8,128)(2,1)}, u32[]{:S(2)}) copy-start(bf16[8,2048]{1,0:T(8,128)(2,1)} %param.23) | copy-start | bytes 98308
  50.8 44.6 %copy-start.5 = (f32[2048]{0:T(1024)S(1)}, f32[2048]{0:T(1024)}, u32[]{:S(2)}) copy-start(f32[2048]{0:T(1024)} %param.36) | copy-start | bytes 24580
  113.3 3.5 %copy-start.1 = (bf16[32,8,2048]{2,1,0:T(8,128)(2,1)S(1)}, bf16[32,8,2048]{2,1,0:T(8,128)(2,1)}, u32[]{:S(2)}) copy-start(bf16[32,8,2048]{2,1,0:T(8,128)(2,1)} %gather_5.1) | copy-start | bytes 3145732

commit v2 on v1

v2 whole, which is shorter than its diff:
```python
import functools

import jax
import jax.numpy as jnp
from jax import lax
from jax.experimental import pallas as pl
from jax.experimental.pallas import tpu as pltpu
from jax.sharding import PartitionSpec as P

EPS = 1e-06
VMEM = pltpu.VMEM
MESH = pl.DeviceIdType.MESH


def rms_scale(values, gain):
    return values * lax.rsqrt(jnp.mean(values * values, axis=-1, keepdims=True) + EPS) * gain


def grid_of(count):
    for depth in (4, 2, 1):
        side = int(round((count / depth) ** 0.5))
        if depth * side * side == count:
            return depth, side
    return count, 1


def place(count):
    depth, side = grid_of(count)
    ep = lax.axis_index("ep")
    t = lax.axis_index("tp")
    z = ep // (side * side)
    y = (ep // side) % side
    x = ep % side
    a = x * (1 - t) + y * t
    b = y * (1 - t) + x * t
    return depth, side, t, z, b, a


def ep_of(side, t, z, b, a):
    y = b * (1 - t) + a * t
    x = a * (1 - t) + b * t
    return (z * side + y) * side + x


def near(count):
    depth, side, t, z, b, a = place(count)
    steps = [(lax.rem(z + i, depth), b, a) for i in range(1, depth)]
    steps += [(z, lax.rem(b + i, side), a) for i in range(1, side)]
    steps += [(z, b, lax.rem(a + i, side)) for i in range(1, side)]
    return [(ep_of(side, t, *c), t) for c in steps]


def gather_phase(count, both, block_ref, out_ref, send_sem, recv_sem):
    depth, side, t, z, b, a = place(count)
    zs = [((lax.rem(z + i, depth)), b, a) for i in range(1, depth)]
    bs = [(z, lax.rem(b + i, side), a) for i in range(1, side)]
    as_ = [(z, b, lax.rem(a + i, side)) for i in range(1, side)]
    device_of = lambda c: (ep_of(side, t, *c), t)
    partner = (lax.axis_index("ep"), 1 - t)
    width = 2 if both else 1
    slot_of = lambda dz, db, da: (
        ep_of(side, t, lax.rem(z + dz, depth), lax.rem(b + db, side), lax.rem(a + da, side)) * width
        + (t if both else 0)
    )
    mine = slot_of(0, 0, 0)
    out_ref[mine] = block_ref[...]
    counter = [0]
    started = []
    arrivals = {}

    def send(src, offset, key, device):
        number = counter[0]
        counter[0] += 1
        copy = pltpu.make_async_remote_copy(
            src_ref=src,
            dst_ref=out_ref.at[slot_of(*offset)],
            send_sem=send_sem.at[number],
            recv_sem=recv_sem.at[number],
            device_id=device,
            device_id_type=MESH,
        )
        copy.start()
        started.append(copy)
        arrivals[key] = copy

    def relay(offset, legs):
        dz, db, da = offset
        src = block_ref if offset == (0, 0, 0) else out_ref.at[slot_of(*offset)]
        if "a" in legs:
            for i in range(1, side):
                send(src, offset, ("a", (dz, db, (da - i) % side)), device_of(as_[i - 1]))
        if "b" in legs:
            for i in range(1, side):
                send(src, offset, ("b", (dz, (db - i) % side, da)), device_of(bs[i - 1]))
        if "z" in legs:
            for i in range(1, depth):
                send(src, offset, ("z", ((dz - i) % depth, db, da)), device_of(zs[i - 1]))
        if both:
            send(src, offset, ("t", offset), partner)

    relay((0, 0, 0), "zba")
    for dz in range(1, depth):
        arrivals["z", (dz, 0, 0)].wait_recv()
        relay((dz, 0, 0), "ba")
    for dz in range(depth):
        for db in range(1, side):
            arrivals["b", (dz, db, 0)].wait_recv()
            relay((dz, db, 0), "a")
    for dz in range(depth):
        for db in range(side):
            for da in range(1, side):
                arrivals["a", (dz, db, da)].wait_recv()
                relay((dz, db, da), "")
    if both:
        for key, copy in arrivals.items():
            if key[0] == "t":
                copy.wait_recv()
    for copy in started:
        copy.wait_send()


def copies_of(count, both):
    return count - 1 + (count if both else 0)


def device_at(count, both, i):
    t = lax.axis_index("tp")
    me = lax.axis_index("ep") * 2 + t if both else lax.axis_index("ep")
    other = lax.rem(me + i, count * 2 if both else count)
    return other, ((other // 2, other % 2) if both else (other, t))


def greet_all(count, both):
    barrier = pltpu.get_barrier_semaphore()

    def hello(i, carry):
        pl.semaphore_signal(
            barrier, inc=1, device_id=device_at(count, both, i)[1], device_id_type=MESH
        )
        return carry

    lax.fori_loop(1, count * 2 if both else count, hello, 0)


def exchange_phase(count, both, blocks_ref, out_ref, send_sem, recv_sem):
    total = count * 2 if both else count
    t = lax.axis_index("tp")
    me = lax.axis_index("ep") * 2 + t if both else lax.axis_index("ep")

    def copy(i):
        other, target = device_at(count, both, i)
        return pltpu.make_async_remote_copy(
            src_ref=blocks_ref.at[other],
            dst_ref=out_ref.at[me],
            send_sem=send_sem.at[i],
            recv_sem=recv_sem.at[i],
            device_id=target,
            device_id_type=MESH,
        )

    def start(i, carry):
        copy(i).start()
        return carry

    def finish(i, carry):
        copy(i).wait()
        return carry

    lax.fori_loop(1, total, start, 0)
    out_ref[me] = blocks_ref[me]
    lax.fori_loop(1, total, finish, 0)


def contract(left, right):
    return lax.dot_general(left, right, (((1,), (1,)), ((), ())), preferred_element_type=jnp.float32)


def flat_rows(ref):
    blocks, rows, width = ref.shape
    return ref[...].astype(jnp.float32).reshape(blocks * rows, width)


def project_kernel(
    count,
    tokens_ref,
    gain_ref,
    wq_ref,
    wk_ref,
    wv_ref,
    wz_ref,
    beta_ref,
    decay_ref,
    out_ref,
    rates_ref,
    own,
    rows,
    blocks,
    send_sem,
    recv_sem,
    send_sem2,
    recv_sem2,
):
    partner = (lax.axis_index("ep"), 1 - lax.axis_index("tp"))
    barrier = pltpu.get_barrier_semaphore()
    pl.semaphore_signal(barrier, inc=1, device_id=partner, device_id_type=MESH)
    greet_all(count, False)
    own[...] = rms_scale(tokens_ref[...].astype(jnp.float32), gain_ref[...]).astype(own.dtype)
    pl.semaphore_wait(barrier, count)
    gather_phase(count, True, own, rows, send_sem, recv_sem)
    flat = flat_rows(rows).astype(jnp.bfloat16)
    heads = beta_ref.shape[0]
    columns = wq_ref.shape[0]
    wide = 4 * columns
    source = lax.broadcasted_iota(jnp.int32, (columns, wide), 0)
    target = lax.broadcasted_iota(jnp.int32, (columns, wide), 1)
    moved = jnp.zeros((flat.shape[0], wide), jnp.float32)
    for p, w_ref in enumerate((wq_ref, wk_ref, wv_ref, wz_ref)):
        piece = contract(flat, w_ref[...]).astype(jnp.bfloat16)
        spot = source % (columns // heads) * (4 * heads) + p * heads + source // (columns // heads)
        order = jnp.where(target == spot, 1.0, 0.0).astype(jnp.bfloat16)
        moved = moved + jnp.dot(piece, order, preferred_element_type=jnp.float32)
    blocks[...] = moved.reshape(blocks.shape).astype(blocks.dtype)
    ep = lax.axis_index("ep")
    seq = jnp.concatenate(
        [rows[2 * ep].astype(jnp.float32), rows[2 * ep + 1].astype(jnp.float32)], axis=0
    ).astype(jnp.bfloat16)
    exchange_phase(count, False, blocks, out_ref, send_sem2, recv_sem2)
    rates_ref[:, :heads] = contract(seq, beta_ref[...])
    rates_ref[:, heads:] = contract(seq, decay_ref[...])


def sems(n):
    return [pltpu.SemaphoreType.DMA((n,)), pltpu.SemaphoreType.DMA((n,))]


def comm_call(kernel, number, out_shape, operands, scratch):
    spec = pl.BlockSpec(memory_space=VMEM)
    return pl.pallas_call(
        kernel,
        out_shape=out_shape,
        in_specs=[spec] * len(operands),
        out_specs=jax.tree.map(lambda _: spec, out_shape),
        scratch_shapes=scratch,
        compiler_params=pltpu.CompilerParams(
            collective_id=number, has_side_effects=True, vmem_limit_bytes=60 * 1024 * 1024
        ),
        name=f"stage_{number}",
    )(*operands)


def mix_kernel(
    count,
    gated_ref,
    w_ref,
    tokens_ref,
    gain_ref,
    resid_ref,
    all_ref,
    rows,
    parts,
    landed,
    own,
    send_sem,
    recv_sem,
    send_sem2,
    recv_sem2,
    send_sem3,
    recv_sem3,
):
    greet_all(count, True)
    pl.semaphore_wait(pltpu.get_barrier_semaphore(), 2 * count - 1)
    gather_phase(count, False, gated_ref, rows, send_sem, recv_sem)
    flat = flat_rows(rows).astype(jnp.bfloat16)
    product = jnp.dot(flat, w_ref[...], preferred_element_type=jnp.float32)
    parts[...] = product.reshape(parts.shape).astype(parts.dtype)
    exchange_phase(count, True, parts, landed, send_sem2, recv_sem2)
    mixed = [
        landed[2 * i].astype(jnp.float32) + landed[2 * i + 1].astype(jnp.float32)
        for i in range(count)
    ]
    resid = tokens_ref[...].astype(jnp.float32) + jnp.concatenate(mixed, axis=1)
    resid_ref[...] = resid
    own[...] = rms_scale(resid, gain_ref[...]).astype(own.dtype)
    gather_phase(count, True, own, all_ref, send_sem3, recv_sem3)


def scatter_phase(
    count, part_ref, core_buf, sum1, a_buf, sum2, b_buf, sum3, z_buf, send_sem, recv_sem
):
    depth, side, t, z, b, a = place(count)
    device_of = lambda dz, db, da: (
        ep_of(side, t, lax.rem(z + dz, depth), lax.rem(b + db, side), lax.rem(a + da, side)),
        t,
    )
    partner = (lax.axis_index("ep"), 1 - t)
    counter = [0]
    started = []

    def send(src, dst, device, number=None):
        if number is None:
            number = count + counter[0]
            counter[0] += 1
        copy = pltpu.make_async_remote_copy(
            src_ref=src,
            dst_ref=dst,
            send_sem=send_sem.at[number],
            recv_sem=recv_sem.at[number],
            device_id=device,
            device_id_type=MESH,
        )
        copy.start()
        started.append(copy)
        return copy

    add = lambda first, *rest: functools.reduce(
        lambda u, v: u + v, [w.astype(jnp.float32) for w in (first,) + rest]
    )
    order = [
        (dz, db, da)
        for da in list(range(1, side)) + [0]
        for db in list(range(1, side)) + [0]
        for dz in list(range(1, depth)) + [0]
    ]
    absolute = lambda dz, db, da: ep_of(
        side, t, lax.rem(z + dz, depth), lax.rem(b + db, side), lax.rem(a + da, side)
    )
    for dz, db, da in order:
        spot = absolute(dz, da, db)
        send(part_ref.at[spot * 2 + 1 - t], core_buf.at[spot], partner, spot)

    def core_arrival(spot):
        return pltpu.make_async_remote_copy(
            src_ref=part_ref.at[spot * 2 + 1 - t],
            dst_ref=core_buf.at[spot],
            send_sem=send_sem.at[spot],
            recv_sem=recv_sem.at[spot],
            device_id=partner,
            device_id_type=MESH,
        )

    a_copies = {}
    for c in order:
        dz, db, da = c
        core_arrival(absolute(*c)).wait_recv()
        total = add(part_ref[absolute(*c) * 2 + t], core_buf[absolute(*c)])
        slot = (da * side + db) * depth + dz
        sum1[slot] = total.astype(sum1.dtype)
        if da:
            a_copies[c] = send(
                sum1.at[slot], a_buf.at[(da * side + db) * depth + dz], device_of(0, 0, da)
            )
    b_copies = {}
    for db in list(range(1, side)) + [0]:
        for dz in list(range(1, depth)) + [0]:
            terms = [sum1[db * depth + dz]]
            for da in range(1, side):
                a_copies[dz, db, da].wait_recv()
                terms.append(a_buf[(da * side + db) * depth + dz])
            sum2[db * depth + dz] = add(*terms).astype(sum2.dtype)
            if db:
                b_copies[dz, db] = send(
                    sum2.at[db * depth + dz], b_buf.at[db * depth + dz], device_of(0, db, 0)
                )
    z_copies = []
    for dz in list(range(1, depth)) + [0]:
        terms = [sum2[dz]]
        for db in range(1, side):
            b_copies[dz, db].wait_recv()
            terms.append(b_buf[db * depth + dz])
        total = add(*terms)
        if dz:
            sum3[dz] = total.astype(sum3.dtype)
            z_copies.append(send(sum3.at[dz], z_buf.at[dz], device_of(dz, 0, 0)))
    for dz in range(1, depth):
        z_copies[dz - 1].wait_recv()
        total = total + z_buf[dz].astype(jnp.float32)
    for copy in started:
        copy.wait_send()
    return total


def moe_kernel(
    count,
    rows_ref,
    resid_ref,
    mix_ref,
    dg_ref,
    du_ref,
    dd_ref,
    eg_ref,
    eu_ref,
    ed_ref,
    ids_ref,
    route_ref,
    out_ref,
    part,
    *rest,
):
    ep = lax.axis_index("ep")
    partner = (ep, 1 - lax.axis_index("tp"))
    barrier = pltpu.get_barrier_semaphore()
    peers = [partner] + near(count)
    for device in peers:
        pl.semaphore_signal(barrier, inc=1, device_id=device, device_id_type=MESH)
    wide = flat_rows(rows_ref)
    total, width = wide.shape
    mix = 1.0 / (1.0 + jnp.exp(-jnp.sum(wide * mix_ref[...], axis=1, keepdims=True)))
    flat = wide.astype(jnp.bfloat16)
    weight = jnp.sum(jnp.where(ids_ref[...] == ep, route_ref[...], 0.0), axis=0, keepdims=True)
    line = lax.broadcasted_iota(jnp.int32, (total, total), 0)
    lane = lax.broadcasted_iota(jnp.int32, (total, total), 1)
    weight = jnp.sum(jnp.where(line == lane, weight, 0.0), axis=1, keepdims=True)

    def hidden(gate, up):
        gate = jnp.dot(flat, gate, preferred_element_type=jnp.float32)
        up = jnp.dot(flat, up, preferred_element_type=jnp.float32)
        return (gate / (1.0 + jnp.exp(-gate)) * up).astype(jnp.bfloat16)

    dense = hidden(dg_ref[...], du_ref[...])
    expert = hidden(eg_ref[...], eu_ref[...])
    step = min(512, width)
    for start in range(0, width, step):
        span = slice(start, start + step)
        term = mix * jnp.dot(dense, dd_ref[:, span], preferred_element_type=jnp.float32)
        term = term + weight * jnp.dot(expert, ed_ref[:, span], preferred_element_type=jnp.float32)
        part[:, :, span] = term.reshape(part.shape[0], part.shape[1], step).astype(part.dtype)
    pl.semaphore_wait(barrier, len(peers))
    total = scatter_phase(count, part, *rest)
    out_ref[...] = (resid_ref[...] + total).astype(out_ref.dtype)


def delta_kernel(
    heads, rate_ref, bias_ref, rates_ref, x_ref, gain_ref, state_ref, gated_ref, new_ref, cols_buf, acc
):
    seq = pl.program_id(0)
    count, wide = x_ref.shape[1:]
    part = wide // (4 * heads)
    size = count * part
    silu = lambda v: v / (1.0 + jnp.exp(-v))
    x = x_ref[0]
    for i in range(part):
        cols_buf[pl.ds(i, count, stride=part), :] = x[:, i * 4 * heads : (i + 1) * 4 * heads]
    cols = cols_buf[...]
    rows = silu(jnp.transpose(cols)[2 * heads :])
    cols = silu(cols)
    cols = cols * lax.rsqrt(jnp.sum(cols * cols, axis=0, keepdims=True) + EPS)
    value, gate = rows[:heads], rows[heads:]
    tall = lambda pick: jnp.concatenate(
        [jnp.full((1, size), pick(h), jnp.float32) for h in range(heads)], axis=0
    )
    beta = 1.0 / (1.0 + jnp.exp(-tall(lambda h: rates_ref[seq, h])))
    pre = tall(lambda h: rates_ref[seq, heads + h] + bias_ref[h])
    soft = jnp.maximum(pre, 0.0) + jnp.log1p(jnp.exp(-jnp.abs(pre)))
    retain = jnp.exp(-tall(lambda h: rate_ref[h]) * soft)
    readouts = []
    for h in range(heads):
        query = cols[:, h : h + 1] * size ** (-0.5)
        key = cols[:, heads + h : heads + h + 1]
        keep = retain[h : h + 1]
        old = state_ref[0, h]
        recalled = jnp.sum(old * key, axis=0, keepdims=True)
        correction = value[h : h + 1] - keep * recalled
        new = keep * old + key * (beta[h : h + 1] * correction)
        new_ref[0, h] = new
        readouts.append(jnp.sum(new * query, axis=0, keepdims=True))
    readout = jnp.concatenate(readouts, axis=0)
    gated = rms_scale(readout, gain_ref[...]) * gate
    acc[pl.ds(pl.multiple_of(seq * heads, heads), heads), :] = gated

    @pl.when(seq == pl.num_programs(0) - 1)
    def _():
        for h in range(heads):
            piece = acc[pl.ds(h, gated_ref.shape[0], stride=heads), :]
            gated_ref[:, h * size : (h + 1) * size] = piece.astype(gated_ref.dtype)


def delta(rate, bias, rates, x, gain, state):
    seqs, heads, size, _ = state.shape
    own = lambda *shape: pl.BlockSpec((1,) + shape, lambda s: (s,) + (0,) * len(shape))
    scalars = pl.BlockSpec(memory_space=pltpu.SMEM)
    return pl.pallas_call(
        functools.partial(delta_kernel, heads),
        grid=(seqs,),
        out_shape=(
            jax.ShapeDtypeStruct((seqs, heads * size), jnp.bfloat16),
            jax.ShapeDtypeStruct(state.shape, state.dtype),
        ),
        in_specs=[
            scalars,
            scalars,
            scalars,
            own(*x.shape[1:]),
            pl.BlockSpec((1, size), lambda s: (0, 0)),
            own(heads, size, size),
        ],
        out_specs=(
            pl.BlockSpec((seqs, heads * size), lambda s: (0, 0)),
            own(heads, size, size),
        ),
        scratch_shapes=[
            pltpu.VMEM((size, 4 * heads), jnp.float32),
            pltpu.VMEM((seqs * heads, size), jnp.float32),
        ],
        compiler_params=pltpu.CompilerParams(dimension_semantics=("arbitrary",)),
        name="delta",
    )(rate, bias, rates, x, gain.reshape(1, size), state)


def body(
    tokens,
    mix_gain,
    w_query,
    w_key,
    w_value,
    w_zgate,
    w_beta,
    w_decay,
    decay_rate,
    decay_bias,
    head_gain,
    state,
    w_out,
    moe_gain,
    dense_mix,
    dense_gate,
    dense_up,
    dense_down,
    expert_gate,
    expert_up,
    expert_down,
    expert_ids,
    route_weight,
):
    count = lax.axis_size("ep")
    own_rows, width = tokens.shape
    seqs, heads, size, _ = state.shape
    total = 2 * count
    narrow, full = jnp.bfloat16, jnp.float32
    turned = [
        w.transpose(1, 2, 0).reshape(-1, width) for w in (w_query, w_key, w_value, w_zgate)
    ]
    wide = 4 * turned[0].shape[0]
    swapped, rates = comm_call(
        functools.partial(project_kernel, count),
        1,
        (
            jax.ShapeDtypeStruct((count, seqs, wide), narrow),
            jax.ShapeDtypeStruct((seqs, 2 * heads), full),
        ),
        [tokens, mix_gain.reshape(1, width)] + turned + [w_beta.T, w_decay.T],
        [
            VMEM((own_rows, width), narrow),
            VMEM((total, own_rows, width), narrow),
            VMEM((count, seqs, wide), narrow),
        ]
        + sems(copies_of(count, True))
        + sems(count),
    )
    x = swapped.astype(full).transpose(1, 0, 2)
    gated, new_state = delta(decay_rate, decay_bias, rates, x, head_gain, state)
    resid, moe_all = comm_call(
        functools.partial(mix_kernel, count),
        2,
        (
            jax.ShapeDtypeStruct((own_rows, width), full),
            jax.ShapeDtypeStruct((total, own_rows, width), narrow),
        ),
        [gated, w_out, tokens, moe_gain.reshape(1, width)],
        [
            VMEM((count, seqs, heads * size), narrow),
            VMEM((total, own_rows, w_out.shape[1]), narrow),
            VMEM((total, own_rows, w_out.shape[1]), narrow),
            VMEM((own_rows, width), narrow),
        ]
        + sems(copies_of(count, False))
        + sems(total)
        + sems(copies_of(count, True)),
    )
    depth, side = grid_of(count)
    copies = count + (side - 1) * side * depth + (side - 1) * depth + depth - 1
    buf = lambda n: VMEM((n, own_rows, width), narrow)
    layer_out = comm_call(
        functools.partial(moe_kernel, count),
        3,
        jax.ShapeDtypeStruct((own_rows, width), narrow),
        [
            moe_all,
            resid,
            dense_mix.astype(full).reshape(1, width),
            dense_gate,
            dense_up,
            dense_down,
            expert_gate[0],
            expert_up[0],
            expert_down[0],
            expert_ids.T,
            route_weight.T,
        ],
        [buf(total)]
        + [buf(count)] * 3
        + [buf(side * depth)] * 2
        + [buf(depth)] * 2
        + sems(copies),
    )
    return (layer_out, new_state)


def solution(mesh):
    placed = (
        P(("ep", "tp"), None),
        P(),
        P(None, "tp", "ep"),
        P(None, "tp", "ep"),
        P(None, "tp", "ep"),
        P(None, "tp", "ep"),
        P(None, "tp"),
        P(None, "tp"),
        P("tp"),
        P("tp"),
        P(),
        P("ep", "tp", None, None),
        P("tp", "ep"),
        P(),
        P(),
        P(None, ("ep", "tp")),
        P(None, ("ep", "tp")),
        P(("ep", "tp"), None),
        P("ep", None, "tp"),
        P("ep", None, "tp"),
        P("ep", "tp", None),
        P(),
        P(),
    )
    return jax.shard_map(
        body,
        mesh=mesh,
        in_specs=placed,
        out_specs=(P(("ep", "tp"), None), P("ep", "tp", None, None)),
        check_vma=False,
    )
```

time: 147 us -> 108 us (0.73)
  matrix products: 18.8 us -> 0 us
  local copies, waits for them, and re-layouts: 13.9 us -> 1.38 us
  other arithmetic: 9.1 us -> 2.92 us
    dot_general x8 -> x0, matrix products: 18.8 us -> none  [the longest x2 8.06 us: branch(): jnp.dot(hidden.astype(jnp.bfloat16), down, preferred_element_type=jnp.flo...]
    transpose x3 -> x0, local copies, waits for them, and re-layouts: 6.7 us -> none  [the longest x2 4.59 us: body(): cols = swapped[:, :, 0].transpose(1, 0, 3, 2).reshape(seqs, size, 2 * heads)]
    convert_element_type x3 -> x0, other arithmetic: 3.61 us -> none  [the longest x1 1.47 us: body(): layer_out = (resid + scatter(terms, ep_count, 6)).astype(jnp.bfloat16)]
    pallas_call x6 -> x3, Pallas kernels: 88 us -> 85.2 us  [comm_call(): pl.pallas_call(kernel, out_shape=out_shape, in_specs=[spec] * len(operand...]
    reduce_sum x4 -> x0, other arithmetic: 2.6 us -> none  [the longest x2 1.02 us: rms_scale(): jnp.mean(values * values, axis=-1, keepdims=True) + EPS]
    convert_element_type x1 -> x0, local copies, waits for them, and re-layouts: 2.57 us -> none  [body(): swapped.reshape(ep_count, seqs, 2, 2 * heads, part).astype(jnp.float32)]
    pallas_call x1, Pallas kernels: 15 us -> 16.8 us  [delta(): pl.pallas_call(functools.partial(delta_kernel, heads), grid=(seqs,), out_...]
    transpose x0 -> x1, other arithmetic: none -> 1.64 us  [body(): x = swapped.astype(full).transpose(1, 0, 2)]
where the time goes in v2:
time: 108 us; the launch traced here: 107 us
  Pallas kernels  102 us (94%)
  other arithmetic  2.92 us (3%)
  local copies, waits for them, and re-layouts  1.38 us (1%)
    pallas_call x3, Pallas kernels, comm_call(): pl.pallas_call(kernel, out_shape=out_shape, in_specs=[spec] * len(operand...  85.2 us
    pallas_call x1, Pallas kernels, delta(): pl.pallas_call(functools.partial(delta_kernel, heads), grid=(seqs,), out_...  16.8 us

profile of v2, /device:TPU:0, one launch (start us, length us, event | category | flops | bytes accessed | tf_op | source)
XLA Modules:
  0.0 107.0 jit_solution(8480468805044729721)
XLA Ops:
  0.6 1.3 %reshape.39 = f32[2048]{0:T(1024)} convert(bf16[2048]{0:T(1024)(128)(2,1)} %param.37) | non-fusion elementwise | flops 2048 | bytes 12288 | tf_op jit(solution)/shard_map/reshape | solution.py:589
  1.9 29.2 %stage_1.1 = (bf16[16,16,256]{2,1,0:T(8,128)(2,1)}, f32[16,16]{1,0:T(8,128)}) custom-call(bf16[8,2048]{1,0:T(8,128)(2,1)} %tokens_ref.3, f32[1,2048]{1,0:T(1,128)} %bitcast.35, bf16[64,2048]{1,0:T(8,128)(2,1)} %bitcast.28, bf16[64,2048]{1,0:T(8,128)(2,1)} %bitcast.29, bf16[64,2048]{1,0:T(8,128)(2,1)} %bitcast.30, bf16[64,2048]{1,0:T(8,128)(2,1)} %bitcast.31, ...), custom_call_target="tpu_custom_call" | custom-call | tf_op jit(solution)/shard_map/stage_1/pallas_call | solution.py:238
  31.1 1.6 %convert_bitcast_fusion.x_ref = f32[16,16,256]{2,1,0:T(8,128)} fusion(bf16[16,16,256]{2,1,0:T(8,128)(2,1)} %get-tuple-element.9), kind=kLoop, calls=%fused_computation | loop fusion | flops 65536 | bytes 393216 | tf_op jit(solution)/shard_map/transpose | solution.py:559
  32.8 16.8 %delta.1 = (bf16[16,1024]{1,0:T(8,128)(2,1)}, f32[16,8,128,128]{3,2,1,0:T(8,128)}) custom-call(f32[8]{0:T(128)} %rate_ref.1, f32[8]{0:T(128)} %bias_ref.1, f32[16,16]{1,0:T(8,128)} %get-tuple-element.8.rates_ref, f32[16,16,256]{2,1,0:T(8,128)} %convert_bitcast_fusion.x_ref, f32[1,128]{1,0:T(1,128)} %bitcast.39, f32[16,8,128,128]{3,2,1,0:T(8,128)} %state_ref.1), custom_call_target="tpu_custom_call" | custom-call | tf_op jit(solution)/shard_map/delta/pallas_call | solution.py:481
  49.5 36.4 %stage_2.1 = (f32[8,2048]{1,0:T(8,128)}, bf16[32,8,2048]{2,1,0:T(8,128)(2,1)}) custom-call(bf16[16,1024]{1,0:T(8,128)(2,1)} %get-tuple-element.10.gated_ref, bf16[1024,128]{1,0:T(8,128)(2,1)} %w_ref.1, bf16[8,2048]{1,0:T(8,128)(2,1)} %tokens_ref.3, f32[1,2048]{1,0:T(1,128)} %bitcast.36), custom_call_target="tpu_custom_call" | custom-call | tf_op jit(solution)/shard_map/stage_2/pallas_call | solution.py:238
  85.9 19.6 %stage_3.1 = bf16[8,2048]{1,0:T(8,128)(2,1)} custom-call(bf16[32,8,2048]{2,1,0:T(8,128)(2,1)} %get-tuple-element.11.rows_ref, f32[8,2048]{1,0:T(8,128)} %get-tuple-element.12.resid_ref, f32[1,2048]{1,0:T(1,128)} %bitcast.34, bf16[2048,128]{1,0:T(8,128)(2,1)} %dg_ref.1, bf16[2048,128]{1,0:T(8,128)(2,1)} %du_ref.1, bf16[128,2048]{1,0:T(8,128)(2,1)} %dd_ref.1, ...), custom_call_target="tpu_custom_call" | custom-call | tf_op jit(solution)/shard_map/stage_3/pallas_call | solution.py:238
  105.6 1.4 %copy.28 = bf16[8,2048]{1,0:T(8,128)(2,1)} copy(bf16[8,2048]{1,0:T(8,128)(2,1)} %stage_3.1) | data formatting | bytes 65536
